TPU v7x, 32 devices: a whole 2x2x4 slice. The times are simulated.
32 devices in a mesh: ep: 16 (over z, y, x), tp: 2 (over core).
Axes of the slice: x: 2, y: 2, z: 4, core: 2. Of those that a mesh axis runs over, the one named last changes fastest.
Arguments:
- tokens: bfloat16 [64, 4096], P('ep'), may hold values from -6 to 6
- memory: float32 [64, 8, 256, 512], P('ep', 'tp'), may hold values from -6 to 6
- normalizer: float32 [64, 8, 256], P('ep', 'tp'), may hold values from -6 to 6
- stabilizer: float32 [64, 8], P('ep', 'tp'), may hold values from -4 to 4
- norm_gain: float32 [4096], replicated, may hold values from 0.1 to 1.9
- w_query: bfloat16 [4096, 8, 256], P(None, 'tp', 'ep'), may hold values from -0.09375 to 0.09375
- w_key: bfloat16 [4096, 8, 256], P(None, 'tp', 'ep'), may hold values from -0.09375 to 0.09375
- w_value: bfloat16 [4096, 8, 512], P(None, 'tp', 'ep'), may hold values from -0.09375 to 0.09375
- w_outgate: bfloat16 [4096, 8, 512], P(None, 'tp', 'ep'), may hold values from -0.09375 to 0.09375
- w_input: bfloat16 [4096, 8], P(None, 'tp'), may hold values from -0.09375 to 0.09375
- w_forget: bfloat16 [4096, 8], P(None, 'tp'), may hold values from -0.09375 to 0.09375
- forget_bias: float32 [8], P('tp'), may hold values from 0 to 4
- w_out: bfloat16 [4096, 4096], P('tp', 'ep'), may hold values from -0.09375 to 0.09375
- ffn_gain: float32 [4096], replicated, may hold values from 0.1 to 1.9
- w_gate: bfloat16 [16, 4096, 512], P('ep', None, 'tp'), may hold values from -0.09375 to 0.09375
- w_up: bfloat16 [16, 4096, 512], P('ep', None, 'tp'), may hold values from -0.09375 to 0.09375
- w_down: bfloat16 [16, 512, 4096], P('ep', 'tp'), may hold values from -0.25 to 0.25
- expert_ids: int32 [64, 2], P('ep'), may hold values from 0 to 15, as said below
- route_weights: float32 [64, 2], P('ep'), may hold values from 0.1 to 1
Outputs:
- out: bfloat16 [64, 4096], P('ep')
- memory_next: float32 [64, 8, 256, 512], P('ep', 'tp')
- normalizer_next: float32 [64, 8, 256], P('ep', 'tp')
- stabilizer_next: float32 [64, 8], P('ep', 'tp')
Inputs may be any that keep to these rules, and one draw needn't show every extreme that they name: `expert_ids`: the 2 experts of a token differ and lie in one group of 8 consecutive experts. Beyond that, any choice is allowed: for instance, all 4 tokens of one index of ep may name the same expert.
All inputs are finite; a program needn't handle non-finite values.
Results may differ from a plain program's by a relative error of at most 0.013.
Values may be sent and summed in bfloat16 or wider, within the bound.
No kernel may reach another device: no remote copies, remote signals or barrier semaphores. Data moves between devices by JAX's collectives and lax.ppermute only.
A program may use at most 128 MiB of HBM per device.

v0:
```python
import jax
import jax.numpy as jnp
from jax import lax
from jax.sharding import PartitionSpec as P


def rms_scale(values, gain):
    return values * lax.rsqrt(jnp.mean(values * values, axis=-1, keepdims=True) + 1e-06) * gain


def product(left, right):
    return jnp.dot(left, right, preferred_element_type=jnp.float32)


def rounded_term(values):
    return lax.optimization_barrier(values.astype(jnp.bfloat16)).astype(jnp.float32)


def body(
    tokens,
    memory,
    normalizer,
    stabilizer,
    norm_gain,
    w_query,
    w_key,
    w_value,
    w_outgate,
    w_input,
    w_forget,
    forget_bias,
    w_out,
    ffn_gain,
    w_gate,
    w_up,
    w_down,
    expert_ids,
    route_weights,
):
    seqs, width = tokens.shape
    heads, key_size, value_size = (memory.shape[1], memory.shape[2], memory.shape[3])
    value_width = heads * value_size
    key_piece = w_query.shape[2]
    value_piece = w_value.shape[2]
    query_cols = w_query.reshape(width, heads * key_piece)
    key_cols = w_key.reshape(width, heads * key_piece)
    value_cols = w_value.reshape(width, heads * value_piece)
    outgate_cols = w_outgate.reshape(width, heads * value_piece)
    normed = rms_scale(tokens.astype(jnp.float32), norm_gain).astype(jnp.bfloat16)
    piece = lax.all_gather(normed, "ep", axis=0, tiled=True)
    projected = jnp.concatenate(
        [
            product(piece, query_cols),
            product(piece, key_cols),
            product(piece, value_cols),
            product(piece, outgate_cols),
        ],
        axis=1,
    ).astype(jnp.bfloat16)
    all_rows = projected.shape[0]
    narrow = heads * key_piece
    broad = heads * value_piece
    query_part = projected[:, :narrow].reshape(all_rows, heads, key_piece)
    key_part = projected[:, narrow : 2 * narrow].reshape(all_rows, heads, key_piece)
    value_part = projected[:, 2 * narrow : 2 * narrow + broad].reshape(all_rows, heads, value_piece)
    outgate_part = projected[:, 2 * narrow + broad :].reshape(all_rows, heads, value_piece)
    query, key, value, outgate = (
        lax.all_to_all(query_part, "ep", split_axis=0, concat_axis=2, tiled=True),
        lax.all_to_all(key_part, "ep", split_axis=0, concat_axis=2, tiled=True),
        lax.all_to_all(value_part, "ep", split_axis=0, concat_axis=2, tiled=True),
        lax.all_to_all(outgate_part, "ep", split_axis=0, concat_axis=2, tiled=True),
    )
    in_pre = product(normed, w_input)
    log_forget = jax.nn.log_sigmoid(product(normed, w_forget) + forget_bias)
    scaled = query.astype(jnp.float32) * key_size ** (-0.5)
    key_heads = key.astype(jnp.float32)
    value_heads = value.astype(jnp.float32)
    stab_next = jnp.maximum(log_forget + stabilizer, in_pre)
    decay = jnp.exp(log_forget + stabilizer - stab_next)
    inweight = jnp.exp(in_pre - stab_next)
    memory_next = decay[:, :, None, None] * memory + inweight[:, :, None, None] * (
        key_heads[:, :, :, None] * value_heads[:, :, None, :]
    )
    normalizer_next = decay[:, :, None] * normalizer + inweight[:, :, None] * key_heads
    numerator = jnp.einsum("shd,shde->she", scaled, memory_next, precision=lax.Precision.HIGHEST)
    denominator = jnp.sum(scaled * normalizer_next, axis=-1)
    hidden = numerator / jnp.maximum(jnp.abs(denominator), jnp.exp(-stab_next))[:, :, None]
    hidden = (
        hidden.reshape(seqs, value_width)
        * jax.nn.sigmoid(outgate.reshape(seqs, value_width).astype(jnp.float32))
    ).astype(jnp.bfloat16)
    partial_value = product(lax.all_gather(hidden, "ep", axis=0, tiled=True), w_out)
    summed = lax.psum(rounded_term(partial_value).astype(jnp.bfloat16), "tp")
    mixed = lax.all_to_all(summed, "ep", split_axis=0, concat_axis=1, tiled=True)
    resid = tokens.astype(jnp.float32) + mixed.astype(jnp.float32)
    ffn_in = rms_scale(resid, ffn_gain).astype(jnp.bfloat16)
    gate_local, up_local, down_local = (w_gate[0], w_up[0], w_down[0])
    n_experts = lax.axis_size("ep") * w_gate.shape[0]
    piece = lax.all_gather(ffn_in, "ep", axis=0, tiled=True)
    gate_part = product(piece, gate_local)
    up_part = product(piece, up_local)
    act = (jax.nn.silu(gate_part) * up_part).astype(jnp.bfloat16)
    expert_terms = rounded_term(product(act, down_local))
    labels = jnp.arange(n_experts, dtype=jnp.int32)
    route_dense = jnp.sum(
        jnp.where(expert_ids[:, :, None] == labels[None, None, :], route_weights[:, :, None], 0.0),
        axis=1,
    )
    my_weight = lax.all_to_all(route_dense, "ep", split_axis=1, concat_axis=0, tiled=True)
    contrib = expert_terms * my_weight
    n_ep = lax.axis_size("ep")
    n_tp = lax.axis_size("tp")
    arranged = jnp.swapaxes(contrib.reshape(n_ep, seqs, n_tp, width // n_tp), 1, 2)
    arranged = arranged.reshape(n_ep * n_tp * seqs, width // n_tp)
    mine = lax.psum_scatter(arranged, ("ep", "tp"), scatter_dimension=0, tiled=True)
    ffn_out = lax.all_gather(mine.astype(jnp.bfloat16), "tp", axis=1, tiled=True).astype(mine.dtype)
    out = (resid + ffn_out).astype(jnp.bfloat16)
    return (out, memory_next, normalizer_next, stab_next)


def solution(mesh):
    return jax.shard_map(
        body,
        mesh=mesh,
        in_specs=(
            P("ep", None),
            P("ep", "tp", None, None),
            P("ep", "tp", None),
            P("ep", "tp"),
            P(),
            P(None, "tp", "ep"),
            P(None, "tp", "ep"),
            P(None, "tp", "ep"),
            P(None, "tp", "ep"),
            P(None, "tp"),
            P(None, "tp"),
            P("tp"),
            P("tp", "ep"),
            P(),
            P("ep", None, "tp"),
            P("ep", None, "tp"),
            P("ep", "tp", None),
            P("ep", None),
            P("ep", None),
        ),
        out_specs=(P("ep", None), P("ep", "tp", None, None), P("ep", "tp", None), P("ep", "tp")),
        check_vma=False,
    )
```

profile of v0, /device:TPU:0, one launch (start us, length us, event | category | flops | bytes accessed | tf_op | source)
XLA Modules:
  0.0 274.0 jit_solution(16929384175384432204)
XLA Ops:
  0.7 1.1 fusion.14
  1.7 0.9 fusion.49
  2.6 45.3 %all-gather = bf16[16,4,4096]{2,1,0:T(4,128)(2,1)S(1)} all-gather(bf16[1,4,4096]{2,1,0:T(4,128)(2,1)S(1)} %fusion.49), channel_id=1, replica_groups=mesh['ep'=16,'tp'=2] {'ep'}, dimensions={0}, use_global_device_ids=true | all-gather | bytes 557056 | tf_op jit(solution)/shard_map/all_gather | solution.py:50
  47.9 0.1 reshape.133
  48.0 1.3 convolution_convert_fusion.4
  49.5 0.1 copy.119
  49.6 0.7 reshape.153
  50.3 3.5 %all-to-all-start.1 = ((bf16[16,2,128]{2,1,0:T(2,128)(2,1)}), bf16[16,2,128]{2,1,0:T(2,128)(2,1)S(1)}, u32[]{:S(2)}, u32[]{:S(2)}) async-start(bf16[16,2,128]{2,1,0:T(2,128)(2,1)} %reshape.153), calls=%async_computation.1 | async-start | bytes 16384 | tf_op jit(solution)/shard_map/all_to_all | solution.py:69
  53.8 0.8 fusion.16
  54.6 0.9 fusion.29
  55.5 0.9 subtract_exponential_fusion.1
  56.5 1.3 convolution_convert_fusion.5
  57.9 1.7 convolution_convert_fusion.3
  59.6 1.7 convolution_convert_fusion.2
  61.3 0.8 select_reduce_fusion
  62.2 0.1 copy.114
  62.3 0.7 reshape.149
  63.0 0.1 copy.122
  63.1 0.1 copy.123
  63.2 0.7 reshape.151
  63.9 0.1 copy.126
  64.1 0.1 copy.127
  64.2 0.7 reshape.155
  64.9 0.7 copy.131
  65.6 6.9 %all-to-all-start = ((bf16[16,2,128]{2,1,0:T(2,128)(2,1)}), bf16[16,2,128]{2,1,0:T(2,128)(2,1)S(1)}, u32[]{:S(2)}, u32[]{:S(2)}) async-start(bf16[16,2,128]{2,1,0:T(2,128)(2,1)} %reshape.149), calls=%async_computation | async-start | bytes 16384 | tf_op jit(solution)/shard_map/all_to_all | solution.py:68
  72.5 0.1 reshape.154
  72.6 0.1 reshape.120
  72.7 7.0 %all-to-all-done = bf16[16,2,128]{2,1,0:T(2,128)(2,1)S(1)} async-done(((bf16[16,2,128]{2,1,0:T(2,128)(2,1)}), bf16[16,2,128]{2,1,0:T(2,128)(2,1)S(1)}, u32[]{:S(2)}, u32[]{:S(2)}) %all-to-all-start) | async-done | bytes 8224 | tf_op jit(solution)/shard_map/all_to_all | solution.py:68
  79.7 3.5 %all-to-all-start.2 = ((bf16[16,2,256]{2,1,0:T(2,128)(2,1)}), bf16[16,2,256]{2,1,0:T(2,128)(2,1)S(1)}, u32[]{:S(2)}, u32[]{:S(2)}) async-start(bf16[16,2,256]{2,1,0:T(2,128)(2,1)} %reshape.151), calls=%async_computation.2 | async-start | bytes 32768 | tf_op jit(solution)/shard_map/all_to_all | solution.py:70
  83.2 0.1 reshape.150
  83.4 0.1 copy.116
  83.5 0.1 mul.130
  83.6 0.7 multiply_reduce_fusion.1
  84.3 0.1 reshape.141
  84.5 6.1 %all-to-all-done.2 = bf16[16,2,256]{2,1,0:T(2,128)(2,1)S(1)} async-done(((bf16[16,2,256]{2,1,0:T(2,128)(2,1)}), bf16[16,2,256]{2,1,0:T(2,128)(2,1)S(1)}, u32[]{:S(2)}, u32[]{:S(2)}) %all-to-all-start.2) | async-done | bytes 16416 | tf_op jit(solution)/shard_map/all_to_all | solution.py:70
  90.6 3.5 %all-to-all-start.3 = ((bf16[16,2,256]{2,1,0:T(2,128)(2,1)}), bf16[16,2,256]{2,1,0:T(2,128)(2,1)S(1)}, u32[]{:S(2)}, u32[]{:S(2)}) async-start(bf16[16,2,256]{2,1,0:T(2,128)(2,1)} %reshape.155), calls=%async_computation.3 | async-start | bytes 32768 | tf_op jit(solution)/shard_map/all_to_all | solution.py:71
  94.0 0.1 reshape.152
  94.2 0.1 reshape.121
  94.3 4.2 %multiply_add_fusion = f32[4,4,256,512]{3,2,1,0:T(8,128)S(1)} fusion(f32[4,4,256,512]{3,2,1,0:T(8,128)} %param.20, f32[4,4,512]{2,1,0:T(4,128)S(1)} %reshape.121, f32[4,4,256]{2,1,0:T(4,128)S(1)} %reshape.120, f32[4,4]{1,0:T(4,128)S(1)} %subtract_exponential_fusion, f32[4,4]{1,0:T(4,128)S(1)} %get-tuple-element.6), kind=kLoop, calls=%fused_computation | loop fusion | flops 8388608 | bytes 16826496 | tf_op jit(solution)/shard_map/add | solution.py:81
  98.5 3.4 %copy-done.1 = f32[4,4,256,512]{3,2,1,0:T(8,128)} copy-done((f32[4,4,256,512]{3,2,1,0:T(8,128)}, f32[4,4,256,512]{3,2,1,0:T(8,128)S(1)}, u32[]{:S(2)}) %copy-start.1) | copy-done | bytes 8388632
  101.9 4.0 %fusion.30 = f32[4,4,1,512]{3,2,1,0:T(1,128)S(1)} fusion(f32[4,4,256,1]{2,3,1,0:T(1,128)S(1)} %reshape.141, f32[4,4,256,512]{3,2,1,0:T(8,128)S(1)} %multiply_add_fusion), kind=kOutput, calls=%fused_computation.57 | convolution fusion | flops 25165824 | bytes 8437760 | tf_op jit(solution)/shard_map/shd,shde->she/dot_general | solution.py:85
  106.1 6.9 %all-to-all-start.5 = ((f32[4,16,1]{0,2,1:T(1,128)}), f32[4,16,1]{0,2,1:T(1,128)S(1)}, u32[]{:S(2)}, u32[]{:S(2)}) async-start(f32[4,16,1]{0,2,1:T(1,128)} %copy.131), calls=%async_computation.5 | async-start | bytes 16384 | tf_op jit(solution)/shard_map/all_to_all | solution.py:109
  113.0 0.1 reshape.156
  113.1 0.1 copy.128
  113.2 0.1 copy.129
  113.3 0.1 reshape.124
  113.5 42.4 %all-gather.1 = bf16[16,4,2048]{2,1,0:T(4,128)(2,1)S(1)} all-gather(bf16[1,4,2048]{2,1,0:T(4,128)(2,1)S(1)} %fusion.25), channel_id=1, replica_groups=mesh['ep'=16,'tp'=2] {'ep'}, dimensions={0}, use_global_device_ids=true | all-gather | bytes 278528 | tf_op jit(solution)/shard_map/all_gather | solution.py:92
  155.8 0.8 reshape.135
  156.6 1.2 convolution_convert_fusion.1
  157.9 4.0 %psum.7 = bf16[16,4,256]{2,1,0:T(4,128)(2,1)} all-reduce(bf16[16,4,256]{2,1,0:T(4,128)(2,1)S(1)} %all_to_all.24), channel_id=1, replica_groups=mesh['ep'=16,'tp'=2] {'tp'}, use_global_device_ids=true, to_apply=%region_2.3 | all-reduce | flops 16384 | bytes 65536 | tf_op jit(solution)/shard_map/psum | solution.py:93
  161.9 3.5 %all-to-all-start.4 = ((bf16[16,4,256]{2,1,0:T(4,128)(2,1)}), bf16[16,4,256]{2,1,0:T(4,128)(2,1)S(1)}, u32[]{:S(2)}, u32[]{:S(2)}) async-start(bf16[16,4,256]{2,1,0:T(4,128)(2,1)} %psum.7), calls=%async_computation.4 | async-start | bytes 65536 | tf_op jit(solution)/shard_map/all_to_all | solution.py:94
  165.5 7.3 %all-to-all-done.4 = bf16[16,4,256]{2,1,0:T(4,128)(2,1)S(1)} async-done(((bf16[16,4,256]{2,1,0:T(4,128)(2,1)}), bf16[16,4,256]{2,1,0:T(4,128)(2,1)S(1)}, u32[]{:S(2)}, u32[]{:S(2)}) %all-to-all-start.4) | async-done | bytes 32800 | tf_op jit(solution)/shard_map/all_to_all | solution.py:94
  172.8 0.1 multiply_reduce_fusion
  173.0 39.4 %all-gather.2 = bf16[16,4,4096]{2,1,0:T(4,128)(2,1)S(1)} all-gather(bf16[1,4,4096]{2,1,0:T(4,128)(2,1)S(1)} %fusion.22), channel_id=1, replica_groups=mesh['ep'=16,'tp'=2] {'ep'}, dimensions={0}, use_global_device_ids=true | all-gather | bytes 557056 | tf_op jit(solution)/shard_map/all_gather | solution.py:99
  212.4 0.1 reshape.137
  212.5 2.0 fusion.3
  214.6 3.8 %convolution_convert_fusion = bf16[64,4096]{1,0:T(8,128)(2,1)} fusion(bf16[1,256,4096]{2,1,0:T(8,128)(2,1)S(1)} %copy-done, bf16[64,4096]{1,0:T(8,128)(2,1)S(1)} %reshape.137, bf16[1,4096,256]{2,1,0:T(8,128)(2,1)} %param.34, f32[64,256]{1,0:T(8,128)S(1)} %fusion.3), kind=kOutput, calls=%fused_computation.1 | convolution fusion | flops 268795904 | bytes 5308416 | tf_op jit(solution)/shard_map/dot_general | solution.py:12
  218.4 1.2 convert_multiply_fusion
  219.6 1.9 reshape.118
  221.4 1.9 copy.132
  223.4 1.3 reshape.119
  224.7 46.8 %all-reduce.2 = bf16[128,2048]{1,0:T(8,128)(2,1)S(1)} all-reduce(f32[128,2048]{1,0:T(8,128)} %reshape.119), channel_id=2, replica_groups=mesh['ep'=16,'tp'=2] {'ep','tp'}, use_global_device_ids=true, to_apply=%region_5.6.clone | all-reduce | flops 262144 | bytes 1572864
  271.5 1.8 all_gather.15
  273.4 0.6 add_convert_fusion
  (42 shorter events, 0.8 us)
Async XLA Ops:
  0.6 214.0 %copy-start = (bf16[1,256,4096]{2,1,0:T(8,128)(2,1)S(1)}, bf16[1,256,4096]{2,1,0:T(8,128)(2,1)}, u32[]{:S(2)}) copy-start(bf16[1,256,4096]{2,1,0:T(8,128)(2,1)} %param.35) | copy-start | bytes 6291460
  0.6 83.0 %copy-start.5 = (f32[4,4,256]{2,1,0:T(4,128)S(1)}, f32[4,4,256]{2,1,0:T(4,128)}, u32[]{:S(2)}) copy-start(f32[4,4,256]{2,1,0:T(4,128)} %param.21) | copy-start | bytes 49156
  50.3 15.3 %all-to-all-start.1 = ((bf16[16,2,128]{2,1,0:T(2,128)(2,1)}), bf16[16,2,128]{2,1,0:T(2,128)(2,1)S(1)}, u32[]{:S(2)}, u32[]{:S(2)}) async-start(bf16[16,2,128]{2,1,0:T(2,128)(2,1)} %reshape.153), calls=%async_computation.1 | async-start | bytes 16384 | tf_op jit(solution)/shard_map/all_to_all | solution.py:69
  56.5 42.0 %copy-start.6 = (f32[4,4]{1,0:T(4,128)}, f32[4,4]{1,0:T(4,128)S(1)}, u32[]{:S(2)}) copy-start(f32[4,4]{1,0:T(4,128)S(1)} %get-tuple-element.7) | copy-start | bytes 196
  65.6 14.1 %all-to-all-start = ((bf16[16,2,128]{2,1,0:T(2,128)(2,1)}), bf16[16,2,128]{2,1,0:T(2,128)(2,1)S(1)}, u32[]{:S(2)}, u32[]{:S(2)}) async-start(bf16[16,2,128]{2,1,0:T(2,128)(2,1)} %reshape.149), calls=%async_computation | async-start | bytes 16384 | tf_op jit(solution)/shard_map/all_to_all | solution.py:68
  79.7 10.9 %all-to-all-start.2 = ((bf16[16,2,256]{2,1,0:T(2,128)(2,1)}), bf16[16,2,256]{2,1,0:T(2,128)(2,1)S(1)}, u32[]{:S(2)}, u32[]{:S(2)}) async-start(bf16[16,2,256]{2,1,0:T(2,128)(2,1)} %reshape.151), calls=%async_computation.2 | async-start | bytes 32768 | tf_op jit(solution)/shard_map/all_to_all | solution.py:70
  90.6 15.5 %all-to-all-start.3 = ((bf16[16,2,256]{2,1,0:T(2,128)(2,1)}), bf16[16,2,256]{2,1,0:T(2,128)(2,1)S(1)}, u32[]{:S(2)}, u32[]{:S(2)}) async-start(bf16[16,2,256]{2,1,0:T(2,128)(2,1)} %reshape.155), calls=%async_computation.3 | async-start | bytes 32768 | tf_op jit(solution)/shard_map/all_to_all | solution.py:71
  98.5 3.4 %copy-start.1 = (f32[4,4,256,512]{3,2,1,0:T(8,128)}, f32[4,4,256,512]{3,2,1,0:T(8,128)S(1)}, u32[]{:S(2)}) copy-start(f32[4,4,256,512]{3,2,1,0:T(8,128)S(1)} %multiply_add_fusion) | copy-start | bytes 25165828
  101.9 54.7 %copy-start.3 = (bf16[2048,256]{1,0:T(8,128)(2,1)S(1)}, bf16[2048,256]{1,0:T(8,128)(2,1)}, u32[]{:S(2)}) copy-start(bf16[2048,256]{1,0:T(8,128)(2,1)} %param.31) | copy-start | bytes 3145732
  101.9 70.8 %copy-start.2 = (bf16[4,4096]{1,0:T(4,128)(2,1)S(1)}, bf16[4,4096]{1,0:T(4,128)(2,1)}, u32[]{:S(2)}) copy-start(bf16[4,4096]{1,0:T(4,128)(2,1)} %param.19) | copy-start | bytes 98308
  101.9 71.0 %copy-start.4 = (f32[4096]{0:T(1024)S(1)}, f32[4096]{0:T(1024)}, u32[]{:S(2)}) copy-start(f32[4096]{0:T(1024)} %param.32) | copy-start | bytes 49156
  106.1 55.8 %all-to-all-start.5 = ((f32[4,16,1]{0,2,1:T(1,128)}), f32[4,16,1]{0,2,1:T(1,128)S(1)}, u32[]{:S(2)}, u32[]{:S(2)}) async-start(f32[4,16,1]{0,2,1:T(1,128)} %copy.131), calls=%async_computation.5 | async-start | bytes 16384 | tf_op jit(solution)/shard_map/all_to_all | solution.py:109
  161.9 10.9 %all-to-all-start.4 = ((bf16[16,4,256]{2,1,0:T(4,128)(2,1)}), bf16[16,4,256]{2,1,0:T(4,128)(2,1)S(1)}, u32[]{:S(2)}, u32[]{:S(2)}) async-start(bf16[16,4,256]{2,1,0:T(4,128)(2,1)} %psum.7), calls=%async_computation.4 | async-start | bytes 65536 | tf_op jit(solution)/shard_map/all_to_all | solution.py:94
where the time goes:
time: 275 us; the launch traced here: 274 us
  blocking collectives  180 us (65%)
  starting transfers between devices  27.7 us (10%)
  waiting for transfers between devices  20.3 us (7%)
  matrix products  19 us (7%)
  local copies, waits for them, and re-layouts  15.6 us (6%)
  other arithmetic  10.7 us (4%)
    unnamed x1, blocking collectives  46.8 us
    all_gather x1, blocking collectives, body(): piece = lax.all_gather(normed, 'ep', axis=0, tiled=True)  45.3 us
    all_gather x1, blocking collectives, body(): lax.all_gather(hidden, 'ep', axis=0, tiled=True)  42.4 us
    all_gather x1, blocking collectives, body(): piece = lax.all_gather(ffn_in, 'ep', axis=0, tiled=True)  39.4 us
    dot_general x9, matrix products, product(): return jnp.dot(left, right, preferred_element_type=jnp.float32)  15 us
    unnamed x26, local copies, waits for them, and re-layouts  7.67 us
    all_to_all x1, waiting for transfers between devices, body(): lax.all_to_all(summed, 'ep', split_axis=0, concat_axis=1, tiled=True)  7.25 us
    all_to_all x1, waiting for transfers between devices, body(): lax.all_to_all(query_part, 'ep', split_axis=0, concat_axis=2, tiled=True)  6.95 us
  transfers between devices with their start and end apart: 6, of which 3 were waited for; matrix products, arithmetic and copies ran while one was open for 9% of the time, Pallas kernels for 0%

commit v1 on v0

--- a/solution.py
+++ b/solution.py
@@ -96,7 +96,14 @@
     ffn_in = rms_scale(resid, ffn_gain).astype(jnp.bfloat16)
     gate_local, up_local, down_local = (w_gate[0], w_up[0], w_down[0])
     n_experts = lax.axis_size("ep") * w_gate.shape[0]
-    piece = lax.all_gather(ffn_in, "ep", axis=0, tiled=True)
+    count = lax.axis_size("ep")
+    route = [(i, (i + 1) % count) for i in range(count)]
+    pieces = [ffn_in]
+    for stride in range(1, count):
+        pieces = [lax.ppermute(pieces[0], "ep", route), *pieces]
+    full = jnp.concatenate(pieces, axis=0)
+    places = (lax.axis_index("ep") + 1) * pieces[-1].shape[0]
+    piece = jnp.roll(full, places, axis=0)
     gate_part = product(piece, gate_local)
     up_part = product(piece, up_local)
     act = (jax.nn.silu(gate_part) * up_part).astype(jnp.bfloat16)

time: 275 us -> 350 us (1.27)
  waiting for transfers between devices: 20.3 us -> 116 us
  blocking collectives: 180 us -> 151 us
  local copies, waits for them, and re-layouts: 15.6 us -> 25 us
    ppermute x0 -> x15, waiting for transfers between devices: none -> 97.7 us  [body(): pieces = [lax.ppermute(pieces[0], 'ep', route), *pieces]]
    all_gather x1 -> x0, blocking collectives: 39.4 us -> none  [body(): piece = lax.all_gather(ffn_in, 'ep', axis=0, tiled=True)]
    all_to_all x0 -> x1, blocking collectives: none -> 9.98 us  [body(): lax.all_to_all(summed, 'ep', split_axis=0, concat_axis=1, tiled=True)]
    all_to_all x1 -> x0, waiting for transfers between devices: 7.25 us -> none  [body(): lax.all_to_all(summed, 'ep', split_axis=0, concat_axis=1, tiled=True)]
    concatenate x0 -> x1, local copies, waits for them, and re-layouts: none -> 7.14 us  [body(): piece = jnp.roll(full, places, axis=0)]
    all_to_all x1, waiting for transfers between devices: 0.01 us -> 5.12 us  [body(): lax.all_to_all(route_dense, 'ep', split_axis=1, concat_axis=0, tiled=True)]
    unnamed x26 -> x41, local copies, waits for them, and re-layouts: 7.67 us -> 9.98 us
  transfers between devices with their start and end apart: 6 -> 20, of which waited for: 3 -> 17; matrix products, arithmetic and copies ran while one was open for 9% -> 6% of each run, Pallas kernels for 0% -> 0%
where the time goes in v1:
time: 350 us; the launch traced here: 349 us
  blocking collectives  151 us (43%)
  waiting for transfers between devices  116 us (33%)
  starting transfers between devices  27.2 us (8%)
  local copies, waits for them, and re-layouts  25 us (7%)
  matrix products  19.1 us (5%)
  other arithmetic  9.97 us (3%)
    ppermute x15, waiting for transfers between devices, body(): pieces = [lax.ppermute(pieces[0], 'ep', route), *pieces]  97.7 us
    unnamed x1, blocking collectives  47.6 us
    all_gather x1, blocking collectives, body(): piece = lax.all_gather(normed, 'ep', axis=0, tiled=True)  45.3 us
    all_gather x1, blocking collectives, body(): lax.all_gather(hidden, 'ep', axis=0, tiled=True)  42.3 us
    dot_general x9, matrix products, product(): return jnp.dot(left, right, preferred_element_type=jnp.float32)  15 us
    unnamed x41, local copies, waits for them, and re-layouts  9.98 us
    all_to_all x1, blocking collectives, body(): lax.all_to_all(summed, 'ep', split_axis=0, concat_axis=1, tiled=True)  9.98 us
    concatenate x1, local copies, waits for them, and re-layouts, body(): piece = jnp.roll(full, places, axis=0)  7.14 us
  transfers between devices with their start and end apart: 20, of which 17 were waited for; matrix products, arithmetic and copies ran while one was open for 6% of the time, Pallas kernels for 0%

profile of v1, /device:TPU:0, one launch (start us, length us, event | category | flops | bytes accessed | tf_op | source)
XLA Modules:
  0.0 348.7 jit_solution(7149659562116120236)
XLA Ops:
  0.7 1.1 fusion.8
  1.7 0.9 fusion.46
  2.6 45.3 %all-gather = bf16[16,4,4096]{2,1,0:T(4,128)(2,1)S(1)} all-gather(bf16[1,4,4096]{2,1,0:T(4,128)(2,1)S(1)} %fusion.46), channel_id=1, replica_groups=mesh['ep'=16,'tp'=2] {'ep'}, dimensions={0}, use_global_device_ids=true | all-gather | bytes 557056 | tf_op jit(solution)/shard_map/all_gather | solution.py:50
  48.0 1.3 convolution_convert_fusion.4
  49.5 0.1 copy.119
  49.6 0.7 reshape.151
  50.3 3.5 all-to-all-start.1
  53.8 0.8 fusion.10
  54.6 1.3 convolution_convert_fusion.5
  56.0 1.7 convolution_convert_fusion.3
  57.7 1.7 convolution_convert_fusion.2
  59.4 0.9 fusion.28
  60.3 1.0 subtract_exponential_fusion.1
  61.5 0.7 reshape.147
  62.5 0.7 reshape.149
  63.4 0.7 reshape.153
  64.1 6.9 %all-to-all-start = ((bf16[16,2,128]{2,1,0:T(2,128)(2,1)}), bf16[16,2,128]{2,1,0:T(2,128)(2,1)S(1)}, u32[]{:S(2)}, u32[]{:S(2)}) async-start(bf16[16,2,128]{2,1,0:T(2,128)(2,1)} %reshape.147), calls=%async_computation | async-start | bytes 16384 | tf_op jit(solution)/shard_map/all_to_all | solution.py:68
  71.3 7.0 %all-to-all-done = bf16[16,2,128]{2,1,0:T(2,128)(2,1)S(1)} async-done(((bf16[16,2,128]{2,1,0:T(2,128)(2,1)}), bf16[16,2,128]{2,1,0:T(2,128)(2,1)S(1)}, u32[]{:S(2)}, u32[]{:S(2)}) %all-to-all-start) | async-done | bytes 8224 | tf_op jit(solution)/shard_map/all_to_all | solution.py:68
  78.2 3.5 %all-to-all-start.2 = ((bf16[16,2,256]{2,1,0:T(2,128)(2,1)}), bf16[16,2,256]{2,1,0:T(2,128)(2,1)S(1)}, u32[]{:S(2)}, u32[]{:S(2)}) async-start(bf16[16,2,256]{2,1,0:T(2,128)(2,1)} %reshape.149), calls=%async_computation.2 | async-start | bytes 32768 | tf_op jit(solution)/shard_map/all_to_all | solution.py:70
  82.2 0.7 multiply_reduce_fusion.1
  83.0 6.1 %all-to-all-done.2 = bf16[16,2,256]{2,1,0:T(2,128)(2,1)S(1)} async-done(((bf16[16,2,256]{2,1,0:T(2,128)(2,1)}), bf16[16,2,256]{2,1,0:T(2,128)(2,1)S(1)}, u32[]{:S(2)}, u32[]{:S(2)}) %all-to-all-start.2) | async-done | bytes 16416 | tf_op jit(solution)/shard_map/all_to_all | solution.py:70
  89.1 3.4 all-to-all-start.3
  92.8 4.2 %multiply_add_fusion = f32[4,4,256,512]{3,2,1,0:T(8,128)S(1)} fusion(f32[4,4,256,512]{3,2,1,0:T(8,128)} %param.20, f32[4,4,512]{2,1,0:T(4,128)S(1)} %reshape.121, f32[4,4,256]{2,1,0:T(4,128)S(1)} %reshape.120, f32[4,4]{1,0:T(4,128)S(1)} %subtract_exponential_fusion, f32[4,4]{1,0:T(4,128)S(1)} %get-tuple-element.6), kind=kLoop, calls=%fused_computation | loop fusion | flops 8388608 | bytes 16826496 | tf_op jit(solution)/shard_map/add | solution.py:81
  97.0 3.4 copy-done.1
  100.4 4.0 %fusion.29 = f32[4,4,1,512]{3,2,1,0:T(1,128)S(1)} fusion(f32[4,4,256,1]{2,3,1,0:T(1,128)S(1)} %reshape.139, f32[4,4,256,512]{3,2,1,0:T(8,128)S(1)} %multiply_add_fusion), kind=kOutput, calls=%fused_computation.54 | convolution fusion | flops 25165824 | bytes 8437760 | tf_op jit(solution)/shard_map/shd,shde->she/dot_general | solution.py:85
  105.1 42.3 %all-gather.1 = bf16[16,4,2048]{2,1,0:T(4,128)(2,1)S(1)} all-gather(bf16[1,4,2048]{2,1,0:T(4,128)(2,1)S(1)} %fusion.21), channel_id=1, replica_groups=mesh['ep'=16,'tp'=2] {'ep'}, dimensions={0}, use_global_device_ids=true | all-gather | bytes 278528 | tf_op jit(solution)/shard_map/all_gather | solution.py:92
  147.4 0.8 reshape.135
  148.2 1.2 convolution_convert_fusion.1
  149.5 3.4 psum.7
  152.9 10.0 %all_to_all.65 = bf16[16,4,256]{2,1,0:T(4,128)(2,1)S(1)} all-to-all(bf16[16,4,256]{2,1,0:T(4,128)(2,1)S(1)} %psum.7), channel_id=1, replica_groups=mesh['ep'=16,'tp'=2] {'ep'}, dimensions={0} | all-to-all | bytes 65536 | tf_op jit(solution)/shard_map/all_to_all | solution.py:94
  162.9 0.1 multiply_reduce_fusion
  163.1 0.7 collective-permute-start
  163.9 6.8 %collective-permute-done = bf16[4,4096]{1,0:T(4,128)(2,1)S(1)} collective-permute-done((bf16[4,4096]{1,0:T(4,128)(2,1)S(1)}, bf16[4,4096]{1,0:T(4,128)(2,1)S(1)}, u32[]{:S(2)}, u32[]{:S(2)}) %collective-permute-start) | collective-permute-done | bytes 32800 | tf_op jit(solution)/shard_map/ppermute | solution.py:103
  170.7 7.5 %collective-permute-done.1 = bf16[4,4096]{1,0:T(4,128)(2,1)S(1)} collective-permute-done((bf16[4,4096]{1,0:T(4,128)(2,1)S(1)}, bf16[4,4096]{1,0:T(4,128)(2,1)S(1)}, u32[]{:S(2)}, u32[]{:S(2)}) %collective-permute-start.1) | collective-permute-done | bytes 32800 | tf_op jit(solution)/shard_map/ppermute | solution.py:103
  178.2 7.5 %collective-permute-done.2 = bf16[4,4096]{1,0:T(4,128)(2,1)S(1)} collective-permute-done((bf16[4,4096]{1,0:T(4,128)(2,1)S(1)}, bf16[4,4096]{1,0:T(4,128)(2,1)S(1)}, u32[]{:S(2)}, u32[]{:S(2)}) %collective-permute-start.2) | collective-permute-done | bytes 32800 | tf_op jit(solution)/shard_map/ppermute | solution.py:103
  185.7 7.5 %collective-permute-done.3 = bf16[4,4096]{1,0:T(4,128)(2,1)S(1)} collective-permute-done((bf16[4,4096]{1,0:T(4,128)(2,1)S(1)}, bf16[4,4096]{1,0:T(4,128)(2,1)S(1)}, u32[]{:S(2)}, u32[]{:S(2)}) %collective-permute-start.3) | collective-permute-done | bytes 32800 | tf_op jit(solution)/shard_map/ppermute | solution.py:103
  193.2 7.8 %collective-permute-done.4 = bf16[4,4096]{1,0:T(4,128)(2,1)S(1)} collective-permute-done((bf16[4,4096]{1,0:T(4,128)(2,1)S(1)}, bf16[4,4096]{1,0:T(4,128)(2,1)S(1)}, u32[]{:S(2)}, u32[]{:S(2)}) %collective-permute-start.4) | collective-permute-done | bytes 32800 | tf_op jit(solution)/shard_map/ppermute | solution.py:103
  201.1 7.5 %collective-permute-done.5 = bf16[4,4096]{1,0:T(4,128)(2,1)S(1)} collective-permute-done((bf16[4,4096]{1,0:T(4,128)(2,1)S(1)}, bf16[4,4096]{1,0:T(4,128)(2,1)S(1)}, u32[]{:S(2)}, u32[]{:S(2)}) %collective-permute-start.5) | collective-permute-done | bytes 32800 | tf_op jit(solution)/shard_map/ppermute | solution.py:103
  208.6 7.5 %collective-permute-done.6 = bf16[4,4096]{1,0:T(4,128)(2,1)S(1)} collective-permute-done((bf16[4,4096]{1,0:T(4,128)(2,1)S(1)}, bf16[4,4096]{1,0:T(4,128)(2,1)S(1)}, u32[]{:S(2)}, u32[]{:S(2)}) %collective-permute-start.6) | collective-permute-done | bytes 32800 | tf_op jit(solution)/shard_map/ppermute | solution.py:103
  216.1 7.5 %collective-permute-done.7 = bf16[4,4096]{1,0:T(4,128)(2,1)S(1)} collective-permute-done((bf16[4,4096]{1,0:T(4,128)(2,1)S(1)}, bf16[4,4096]{1,0:T(4,128)(2,1)S(1)}, u32[]{:S(2)}, u32[]{:S(2)}) %collective-permute-start.7) | collective-permute-done | bytes 32800 | tf_op jit(solution)/shard_map/ppermute | solution.py:103
  223.6 7.5 %collective-permute-done.8 = bf16[4,4096]{1,0:T(4,128)(2,1)S(1)} collective-permute-done((bf16[4,4096]{1,0:T(4,128)(2,1)S(1)}, bf16[4,4096]{1,0:T(4,128)(2,1)S(1)}, u32[]{:S(2)}, u32[]{:S(2)}) %collective-permute-start.8) | collective-permute-done | bytes 32800 | tf_op jit(solution)/shard_map/ppermute | solution.py:103
  231.1 0.6 copy-done.4
  231.7 7.5 %collective-permute-done.9 = bf16[4,4096]{1,0:T(4,128)(2,1)S(1)} collective-permute-done((bf16[4,4096]{1,0:T(4,128)(2,1)S(1)}, bf16[4,4096]{1,0:T(4,128)(2,1)S(1)}, u32[]{:S(2)}, u32[]{:S(2)}) %collective-permute-start.9) | collective-permute-done | bytes 32800 | tf_op jit(solution)/shard_map/ppermute | solution.py:103
  239.2 0.6 copy-done.5
  239.8 7.5 %collective-permute-done.10 = bf16[4,4096]{1,0:T(4,128)(2,1)S(1)} collective-permute-done((bf16[4,4096]{1,0:T(4,128)(2,1)S(1)}, bf16[4,4096]{1,0:T(4,128)(2,1)S(1)}, u32[]{:S(2)}, u32[]{:S(2)}) %collective-permute-start.10) | collective-permute-done | bytes 32800 | tf_op jit(solution)/shard_map/ppermute | solution.py:103
  247.3 0.6 copy-done.6
  247.9 7.5 %collective-permute-done.11 = bf16[4,4096]{1,0:T(4,128)(2,1)S(1)} collective-permute-done((bf16[4,4096]{1,0:T(4,128)(2,1)S(1)}, bf16[4,4096]{1,0:T(4,128)(2,1)S(1)}, u32[]{:S(2)}, u32[]{:S(2)}) %collective-permute-start.11) | collective-permute-done | bytes 32800 | tf_op jit(solution)/shard_map/ppermute | solution.py:103
  255.5 0.6 copy-done.7
  256.1 7.5 %collective-permute-done.12 = bf16[4,4096]{1,0:T(4,128)(2,1)S(1)} collective-permute-done((bf16[4,4096]{1,0:T(4,128)(2,1)S(1)}, bf16[4,4096]{1,0:T(4,128)(2,1)S(1)}, u32[]{:S(2)}, u32[]{:S(2)}) %collective-permute-start.12) | collective-permute-done | bytes 32800 | tf_op jit(solution)/shard_map/ppermute | solution.py:103
  263.7 0.7 copy.131
  264.3 7.0 %all-to-all-start.5 = ((f32[4,16,1]{0,2,1:T(1,128)}), f32[4,16,1]{0,2,1:T(1,128)S(1)}, u32[]{:S(2)}, u32[]{:S(2)}) async-start(f32[4,16,1]{0,2,1:T(1,128)} %copy.131), calls=%async_computation.5 | async-start | bytes 16384 | tf_op jit(solution)/shard_map/all_to_all | solution.py:116
  271.4 2.1 collective-permute-start.14
  273.5 5.1 %all-to-all-done.5 = f32[4,16,1]{0,2,1:T(1,128)S(1)} async-done(((f32[4,16,1]{0,2,1:T(1,128)}), f32[4,16,1]{0,2,1:T(1,128)S(1)}, u32[]{:S(2)}, u32[]{:S(2)}) %all-to-all-start.5) | async-done | bytes 288 | tf_op jit(solution)/shard_map/all_to_all | solution.py:116
  278.8 0.5 collective-permute-done.14
  279.2 7.1 %concatenate.8 = bf16[128,4096]{1,0:T(8,128)(2,1)S(1)} concatenate(bf16[4,4096]{1,0:T(4,128)(2,1)} %collective-permute-done.14, bf16[4,4096]{1,0:T(4,128)(2,1)} %copy-done.9, bf16[4,4096]{1,0:T(4,128)(2,1)} %copy-done.8, bf16[4,4096]{1,0:T(4,128)(2,1)} %copy-done.7, bf16[4,4096]{1,0:T(4,128)(2,1)} %copy-done.6, bf16[4,4096]{1,0:T(4,128)(2,1)} %copy-done.5, ...), dimensions={0} | concatenate | bytes 2097152 | tf_op jit(solution)/shard_map/jit(_roll_dynamic)/concatenate | solution.py:106
  286.4 2.0 fusion.1
  288.4 3.8 %convolution_convert_fusion = bf16[64,4096]{1,0:T(8,128)(2,1)} fusion(bf16[1,256,4096]{2,1,0:T(8,128)(2,1)S(1)} %copy-done, f32[64,256]{1,0:T(8,128)S(1)} %fusion.1, bf16[1,4096,256]{2,1,0:T(8,128)(2,1)} %param.33, bf16[128,4096]{1,0:T(8,128)(2,1)S(1)} %concatenate.8, s32[]{:T(128)S(6)} %select_n.24), kind=kOutput, calls=%fused_computation.1 | convolution fusion | flops 268795904 | bytes 5308420 | tf_op jit(solution)/shard_map/dot_general | solution.py:12
  292.2 1.2 convert_multiply_fusion
  293.4 1.9 reshape.118
  295.3 1.9 copy.132
  297.2 1.3 reshape.119
  298.6 47.6 %all-reduce.2 = bf16[128,2048]{1,0:T(8,128)(2,1)S(1)} all-reduce(f32[128,2048]{1,0:T(8,128)} %reshape.119), channel_id=2, replica_groups=mesh['ep'=16,'tp'=2] {'ep','tp'}, use_global_device_ids=true, to_apply=%region_5.6.clone | all-reduce | flops 262144 | bytes 1572864
  346.2 1.8 all_gather.11
  348.1 0.6 add_convert_fusion
  (86 shorter events, 2.9 us)
Async XLA Ops:
  0.6 287.8 %copy-start = (bf16[1,256,4096]{2,1,0:T(8,128)(2,1)S(1)}, bf16[1,256,4096]{2,1,0:T(8,128)(2,1)}, u32[]{:S(2)}) copy-start(bf16[1,256,4096]{2,1,0:T(8,128)(2,1)} %param.35) | copy-start | bytes 6291460
  0.6 81.5 %copy-start.11 = (f32[4,4,256]{2,1,0:T(4,128)S(1)}, f32[4,4,256]{2,1,0:T(4,128)}, u32[]{:S(2)}) copy-start(f32[4,4,256]{2,1,0:T(4,128)} %param.21) | copy-start | bytes 49156
  50.3 13.8 %all-to-all-start.1 = ((bf16[16,2,128]{2,1,0:T(2,128)(2,1)}), bf16[16,2,128]{2,1,0:T(2,128)(2,1)S(1)}, u32[]{:S(2)}, u32[]{:S(2)}) async-start(bf16[16,2,128]{2,1,0:T(2,128)(2,1)} %reshape.151), calls=%async_computation.1 | async-start | bytes 16384 | tf_op jit(solution)/shard_map/all_to_all | solution.py:69
  61.3 35.7 %copy-start.12 = (f32[4,4]{1,0:T(4,128)}, f32[4,4]{1,0:T(4,128)S(1)}, u32[]{:S(2)}) copy-start(f32[4,4]{1,0:T(4,128)S(1)} %get-tuple-element.7) | copy-start | bytes 196
  64.1 14.1 %all-to-all-start = ((bf16[16,2,128]{2,1,0:T(2,128)(2,1)}), bf16[16,2,128]{2,1,0:T(2,128)(2,1)S(1)}, u32[]{:S(2)}, u32[]{:S(2)}) async-start(bf16[16,2,128]{2,1,0:T(2,128)(2,1)} %reshape.147), calls=%async_computation | async-start | bytes 16384 | tf_op jit(solution)/shard_map/all_to_all | solution.py:68
  78.2 10.8 %all-to-all-start.2 = ((bf16[16,2,256]{2,1,0:T(2,128)(2,1)}), bf16[16,2,256]{2,1,0:T(2,128)(2,1)S(1)}, u32[]{:S(2)}, u32[]{:S(2)}) async-start(bf16[16,2,256]{2,1,0:T(2,128)(2,1)} %reshape.149), calls=%async_computation.2 | async-start | bytes 32768 | tf_op jit(solution)/shard_map/all_to_all | solution.py:70
  89.1 15.5 %all-to-all-start.3 = ((bf16[16,2,256]{2,1,0:T(2,128)(2,1)}), bf16[16,2,256]{2,1,0:T(2,128)(2,1)S(1)}, u32[]{:S(2)}, u32[]{:S(2)}) async-start(bf16[16,2,256]{2,1,0:T(2,128)(2,1)} %reshape.153), calls=%async_computation.3 | async-start | bytes 32768 | tf_op jit(solution)/shard_map/all_to_all | solution.py:71
  97.0 3.4 copy-start.1
  100.4 47.8 %copy-start.3 = (bf16[2048,256]{1,0:T(8,128)(2,1)S(1)}, bf16[2048,256]{1,0:T(8,128)(2,1)}, u32[]{:S(2)}) copy-start(bf16[2048,256]{1,0:T(8,128)(2,1)} %param.31) | copy-start | bytes 3145732
  100.4 62.5 %copy-start.2 = (bf16[4,4096]{1,0:T(4,128)(2,1)S(1)}, bf16[4,4096]{1,0:T(4,128)(2,1)}, u32[]{:S(2)}) copy-start(bf16[4,4096]{1,0:T(4,128)(2,1)} %param.19) | copy-start | bytes 98308
  100.4 62.6 %copy-start.10 = (f32[4096]{0:T(1024)S(1)}, f32[4096]{0:T(1024)}, u32[]{:S(2)}) copy-start(f32[4096]{0:T(1024)} %param.32) | copy-start | bytes 49156
  100.4 163.2 %copy-start.13 = (f32[4,2]{0,1:T(2,128)S(1)}, f32[4,2]{0,1:T(2,128)}, u32[]{:S(2)}) copy-start(f32[4,2]{0,1:T(2,128)} %param.37) | copy-start | bytes 100
  100.4 163.2 %copy-start.14 = (s32[4,2]{0,1:T(2,128)S(1)}, s32[4,2]{0,1:T(2,128)}, u32[]{:S(2)}) copy-start(s32[4,2]{0,1:T(2,128)} %param.36) | copy-start | bytes 100
  163.1 7.6 %collective-permute-start = (bf16[4,4096]{1,0:T(4,128)(2,1)S(1)}, bf16[4,4096]{1,0:T(4,128)(2,1)S(1)}, u32[]{:S(2)}, u32[]{:S(2)}) collective-permute-start(bf16[4,4096]{1,0:T(4,128)(2,1)S(1)} %multiply_convert_fusion.1), channel_id=1, source_target_pairs={{0,2},{2,4},{4,6},{6,8},{8,10},{10,12},{12,14},{14,16},{16,18},{18... | collective-permute-start | bytes 98312 | tf_op jit(solution)/shard_map/ppermute | solution.py:103
  170.7 7.5 %collective-permute-start.1 = (bf16[4,4096]{1,0:T(4,128)(2,1)S(1)}, bf16[4,4096]{1,0:T(4,128)(2,1)S(1)}, u32[]{:S(2)}, u32[]{:S(2)}) collective-permute-start(bf16[4,4096]{1,0:T(4,128)(2,1)S(1)} %collective-permute-done), channel_id=1, source_target_pairs={{0,2},{2,4},{4,6},{6,8},{8,10},{10,12},{12,14},{14,16},{16,18},{18... | collective-permute-start | bytes 98312 | tf_op jit(solution)/shard_map/ppermute | solution.py:103
  178.2 7.5 %collective-permute-start.2 = (bf16[4,4096]{1,0:T(4,128)(2,1)S(1)}, bf16[4,4096]{1,0:T(4,128)(2,1)S(1)}, u32[]{:S(2)}, u32[]{:S(2)}) collective-permute-start(bf16[4,4096]{1,0:T(4,128)(2,1)S(1)} %collective-permute-done.1), channel_id=1, source_target_pairs={{0,2},{2,4},{4,6},{6,8},{8,10},{10,12},{12,14},{14,16},{16,18},{18... | collective-permute-start | bytes 98312 | tf_op jit(solution)/shard_map/ppermute | solution.py:103
  185.7 7.5 %collective-permute-start.3 = (bf16[4,4096]{1,0:T(4,128)(2,1)S(1)}, bf16[4,4096]{1,0:T(4,128)(2,1)S(1)}, u32[]{:S(2)}, u32[]{:S(2)}) collective-permute-start(bf16[4,4096]{1,0:T(4,128)(2,1)S(1)} %collective-permute-done.2), channel_id=1, source_target_pairs={{0,2},{2,4},{4,6},{6,8},{8,10},{10,12},{12,14},{14,16},{16,18},{18... | collective-permute-start | bytes 98312 | tf_op jit(solution)/shard_map/ppermute | solution.py:103
  193.2 7.8 %collective-permute-start.4 = (bf16[4,4096]{1,0:T(4,128)(2,1)S(1)}, bf16[4,4096]{1,0:T(4,128)(2,1)S(1)}, u32[]{:S(2)}, u32[]{:S(2)}) collective-permute-start(bf16[4,4096]{1,0:T(4,128)(2,1)S(1)} %collective-permute-done.3), channel_id=1, source_target_pairs={{0,2},{2,4},{4,6},{6,8},{8,10},{10,12},{12,14},{14,16},{16,18},{18... | collective-permute-start | bytes 98312 | tf_op jit(solution)/shard_map/ppermute | solution.py:103
  201.1 7.5 %collective-permute-start.5 = (bf16[4,4096]{1,0:T(4,128)(2,1)S(1)}, bf16[4,4096]{1,0:T(4,128)(2,1)S(1)}, u32[]{:S(2)}, u32[]{:S(2)}) collective-permute-start(bf16[4,4096]{1,0:T(4,128)(2,1)S(1)} %collective-permute-done.4), channel_id=1, source_target_pairs={{0,2},{2,4},{4,6},{6,8},{8,10},{10,12},{12,14},{14,16},{16,18},{18... | collective-permute-start | bytes 98312 | tf_op jit(solution)/shard_map/ppermute | solution.py:103
  208.6 7.5 %collective-permute-start.6 = (bf16[4,4096]{1,0:T(4,128)(2,1)S(1)}, bf16[4,4096]{1,0:T(4,128)(2,1)S(1)}, u32[]{:S(2)}, u32[]{:S(2)}) collective-permute-start(bf16[4,4096]{1,0:T(4,128)(2,1)S(1)} %collective-permute-done.5), channel_id=1, source_target_pairs={{0,2},{2,4},{4,6},{6,8},{8,10},{10,12},{12,14},{14,16},{16,18},{18... | collective-permute-start | bytes 98312 | tf_op jit(solution)/shard_map/ppermute | solution.py:103
  216.1 7.5 %collective-permute-start.7 = (bf16[4,4096]{1,0:T(4,128)(2,1)S(1)}, bf16[4,4096]{1,0:T(4,128)(2,1)S(1)}, u32[]{:S(2)}, u32[]{:S(2)}) collective-permute-start(bf16[4,4096]{1,0:T(4,128)(2,1)S(1)} %collective-permute-done.6), channel_id=1, source_target_pairs={{0,2},{2,4},{4,6},{6,8},{8,10},{10,12},{12,14},{14,16},{16,18},{18... | collective-permute-start | bytes 98312 | tf_op jit(solution)/shard_map/ppermute | solution.py:103
  223.6 7.5 %collective-permute-start.8 = (bf16[4,4096]{1,0:T(4,128)(2,1)S(1)}, bf16[4,4096]{1,0:T(4,128)(2,1)S(1)}, u32[]{:S(2)}, u32[]{:S(2)}) collective-permute-start(bf16[4,4096]{1,0:T(4,128)(2,1)S(1)} %collective-permute-done.7), channel_id=1, source_target_pairs={{0,2},{2,4},{4,6},{6,8},{8,10},{10,12},{12,14},{14,16},{16,18},{18... | collective-permute-start | bytes 98312 | tf_op jit(solution)/shard_map/ppermute | solution.py:103
  231.1 0.6 copy-start.4
  231.7 7.5 %collective-permute-start.9 = (bf16[4,4096]{1,0:T(4,128)(2,1)S(1)}, bf16[4,4096]{1,0:T(4,128)(2,1)S(1)}, u32[]{:S(2)}, u32[]{:S(2)}) collective-permute-start(bf16[4,4096]{1,0:T(4,128)(2,1)S(1)} %collective-permute-done.8), channel_id=1, source_target_pairs={{0,2},{2,4},{4,6},{6,8},{8,10},{10,12},{12,14},{14,16},{16,18},{18... | collective-permute-start | bytes 98312 | tf_op jit(solution)/shard_map/ppermute | solution.py:103
  239.2 0.6 copy-start.5
  239.8 7.5 %collective-permute-start.10 = (bf16[4,4096]{1,0:T(4,128)(2,1)S(1)}, bf16[4,4096]{1,0:T(4,128)(2,1)S(1)}, u32[]{:S(2)}, u32[]{:S(2)}) collective-permute-start(bf16[4,4096]{1,0:T(4,128)(2,1)S(1)} %collective-permute-done.9), channel_id=1, source_target_pairs={{0,2},{2,4},{4,6},{6,8},{8,10},{10,12},{12,14},{14,16},{16,18},{18... | collective-permute-start | bytes 98312 | tf_op jit(solution)/shard_map/ppermute | solution.py:103
  247.3 0.6 copy-start.6
  247.9 7.5 %collective-permute-start.11 = (bf16[4,4096]{1,0:T(4,128)(2,1)S(1)}, bf16[4,4096]{1,0:T(4,128)(2,1)S(1)}, u32[]{:S(2)}, u32[]{:S(2)}) collective-permute-start(bf16[4,4096]{1,0:T(4,128)(2,1)S(1)} %collective-permute-done.10), channel_id=1, source_target_pairs={{0,2},{2,4},{4,6},{6,8},{8,10},{10,12},{12,14},{14,16},{16,18},{18... | collective-permute-start | bytes 98312 | tf_op jit(solution)/shard_map/ppermute | solution.py:103
  255.5 0.6 copy-start.7
  256.1 7.5 %collective-permute-start.12 = (bf16[4,4096]{1,0:T(4,128)(2,1)S(1)}, bf16[4,4096]{1,0:T(4,128)(2,1)S(1)}, u32[]{:S(2)}, u32[]{:S(2)}) collective-permute-start(bf16[4,4096]{1,0:T(4,128)(2,1)S(1)} %collective-permute-done.11), channel_id=1, source_target_pairs={{0,2},{2,4},{4,6},{6,8},{8,10},{10,12},{12,14},{14,16},{16,18},{18... | collective-permute-start | bytes 98312 | tf_op jit(solution)/shard_map/ppermute | solution.py:103
  263.6 15.2 %copy-start.8 = (bf16[4,4096]{1,0:T(4,128)(2,1)}, bf16[4,4096]{1,0:T(4,128)(2,1)S(1)}, u32[]{:S(2)}) copy-start(bf16[4,4096]{1,0:T(4,128)(2,1)S(1)} %collective-permute-done.12) | copy-start | bytes 98308
  263.6 7.8 %collective-permute-start.13 = (bf16[4,4096]{1,0:T(4,128)(2,1)S(1)}, bf16[4,4096]{1,0:T(4,128)(2,1)S(1)}, u32[]{:S(2)}, u32[]{:S(2)}) collective-permute-start(bf16[4,4096]{1,0:T(4,128)(2,1)S(1)} %collective-permute-done.12), channel_id=1, source_target_pairs={{0,2},{2,4},{4,6},{6,8},{8,10},{10,12},{12,14},{14,16},{16,18},{18... | collective-permute-start | bytes 98312 | tf_op jit(solution)/shard_map/ppermute | solution.py:103
  264.3 14.3 %all-to-all-start.5 = ((f32[4,16,1]{0,2,1:T(1,128)}), f32[4,16,1]{0,2,1:T(1,128)S(1)}, u32[]{:S(2)}, u32[]{:S(2)}) async-start(f32[4,16,1]{0,2,1:T(1,128)} %copy.131), calls=%async_computation.5 | async-start | bytes 16384 | tf_op jit(solution)/shard_map/all_to_all | solution.py:116
  271.4 7.4 %copy-start.9 = (bf16[4,4096]{1,0:T(4,128)(2,1)}, bf16[4,4096]{1,0:T(4,128)(2,1)S(1)}, u32[]{:S(2)}) copy-start(bf16[4,4096]{1,0:T(4,128)(2,1)S(1)} %collective-permute-done.13) | copy-start | bytes 98308
  271.4 7.8 %collective-permute-start.14 = (bf16[4,4096]{1,0:T(4,128)(2,1)S(1)}, bf16[4,4096]{1,0:T(4,128)(2,1)}, u32[]{:S(2)}, u32[]{:S(2)}) collective-permute-start(bf16[4,4096]{1,0:T(4,128)(2,1)S(1)} %collective-permute-done.13), channel_id=1, source_target_pairs={{0,2},{2,4},{4,6},{6,8},{8,10},{10,12},{12,14},{14,16},{16,18},{18... | collective-permute-start | bytes 98312 | tf_op jit(solution)/shard_map/ppermute | solution.py:103
